TPU v7x, 32 devices: a whole 2x2x4 slice. The times are simulated.
32 devices in a mesh: kv: 8 (over z, y), tp: 4 (over x, core).
Axes of the slice: x: 2, y: 2, z: 4, core: 2. Of those that a mesh axis runs over, the one named last changes fastest.
Arguments:
- tokens: bfloat16 [4096, 2048], P('kv', 'tp'), may hold values from -9 to 9
- w_query: bfloat16 [2048, 1536], P(None, 'tp'), may hold values from -1 to 1
- w_key: bfloat16 [2048, 1536], P(None, 'tp'), may hold values from -1 to 1
- w_value: bfloat16 [2048, 1536], P(None, 'tp'), may hold values from -0.5 to 0.5
- w_out: bfloat16 [1536, 2048], P('tp'), may hold values from -0.15625 to 0.15625
- chosen: int32 [128, 24], P('kv'), may hold values from 0 to 127, as said below
Outputs:
- mixed: bfloat16 [4096, 2048], P(('kv', 'tp'))
Inputs may be any that keep to these rules, and one draw needn't show every extreme that they name: `chosen`: row c names blocks no later than c; its first entry is c and its second c - 1 (0 for row 0), and an entry may repeat. Taking the rows in aligned runs of 16, one run for each index of kv, the rows of one run name at most 2 distinct blocks lying in any one other index's positions; in every draw some index of kv names exactly 2 from every earlier index. Every run names some block of the index just before it and of the index half the axis before it, where those exist.
All inputs are finite; a program needn't handle non-finite values.
Results may differ from a plain program's by a relative error of at most 0.014.
Values may be sent and summed in bfloat16 or wider, within the bound.
A program may use at most 320 MiB of HBM per device.

v0:
```python
import functools

import jax
import jax.numpy as jnp
from jax import lax
from jax.experimental import pallas as pl
from jax.experimental.pallas import tpu as pltpu
from jax.sharding import PartitionSpec as P

HD = 128
BLK = 32
MOST = 2
NEG = -1e30
LOG2E = 1.4426950408889634
BF = jnp.bfloat16
F32 = jnp.float32
MESH = pl.DeviceIdType.MESH
OWN_CHUNKS = 4
OUT_CHUNKS = 4


def dot(a, b):
    return jnp.dot(a, b, preferred_element_type=F32)


def dot_nt(a, b):
    return lax.dot_general(a, b, (((1,), (1,)), ((), ())), preferred_element_type=F32)


def quot(x, size):
    if size & (size - 1) == 0:
        return lax.shift_right_logical(x, jnp.full(x.shape, size.bit_length() - 1, x.dtype))
    return lax.div(x, size)


def rest(x, size):
    if size & (size - 1) == 0:
        return x & (size - 1)
    return lax.rem(x, size)


def iota(shape, dim):
    return lax.broadcasted_iota(jnp.int32, shape, dim)


def kernel(
    n, tok, wq, wk, wv, wo, chosen, out,
    wbuf, wobuf, gat, far, pick, ask, asked, acc, accf, qb, kb, vb, kf, vf,
    bias, biasf, top, tot, summed, att, psend, precv, xsend, xrecv, mine,
    wsem, ox_s, ox_r, oc_s, oc_r, of_s, of_r, rq_s, rq_r, fk_s, fk_r,
    fx_s, fx_r, fc_s, fc_r, ff_s, ff_r, pd_s, pd_r, px_s, px_r,
):
    rows, feat = tok.shape
    width = wq.shape[1]
    heads = width // HD
    per = rows // BLK
    blocks = n * per
    slot = MOST * BLK
    cols = wo.shape[1]
    quarter = rows // 4
    me = lax.axis_index("kv")
    t = lax.axis_index("tp")
    mate = t + 1 - 2 * lax.rem(t, 2)
    across = lax.rem(t + 2, 4)
    diag = lax.rem(mate + 2, 4)
    order = (t, mate, across, diag)

    loads = []
    for d in range(4):
        for j, w in enumerate((wq, wk, wv)):
            src = pl.ds(pl.multiple_of(order[d] * feat, feat), feat)
            c = pltpu.make_async_copy(w.at[src, :], wbuf.at[j, d], wsem.at[d * 3 + j])
            c.start()
            loads.append(c)
    wo_load = pltpu.make_async_copy(wo, wobuf, wsem.at[12])
    wo_load.start()

    barrier = pltpu.get_barrier_semaphore()
    for d in range(1, 4):
        pl.semaphore_signal(barrier, inc=1, device_id=(me, order[d]), device_id_type=MESH)
    for k in range(1, n):
        pl.semaphore_signal(
            barrier, inc=1, device_id=(lax.rem(me + k, n), t), device_id_type=MESH
        )
    pl.semaphore_wait(barrier, n + 2)

    def remote(src, dst, s, r, who):
        c = pltpu.make_async_remote_copy(
            src_ref=src, dst_ref=dst, send_sem=s, recv_sem=r, device_id=who, device_id_type=MESH
        )
        return c

    piece = rows // OWN_CHUNKS
    own_x = []
    for c in range(OWN_CHUNKS):
        part = pl.ds(c * piece, piece)
        own_x.append(
            remote(tok.at[part], gat.at[1, part], ox_s.at[c], ox_r.at[c], (me, across))
        )
        own_x[-1].start()
    own_c = remote(tok, gat.at[0], oc_s, oc_r, (me, mate))
    own_c.start()

    lane = iota((per, blocks), 1)
    seen = jnp.zeros((per, blocks), jnp.int32)
    picks = chosen[...]
    for j in range(picks.shape[1]):
        seen = jnp.maximum(seen, (picks[:, j : j + 1] == lane).astype(jnp.int32))
    wanted = jnp.max(seen, axis=0, keepdims=True)
    lane1 = iota((1, blocks), 1)
    inside = (lane1 >= me * per) & (lane1 < me * per + per)
    wanted = jnp.where(inside, 0, wanted)
    ask[...] = jnp.broadcast_to(wanted, (8, blocks))
    asks = []
    for k in range(1, n):
        c = remote(
            ask, asked.at[k - 1], rq_s.at[k - 1], rq_r.at[k - 1], (lax.rem(me + n - k, n), t)
        )
        c.start()
        asks.append(c)

    ia, ib = iota((blocks, blocks), 0), iota((blocks, blocks), 1)
    tri = ((quot(ia, per) == quot(ib, per)) & (ia <= ib)).astype(BF)
    seen_b = seen.astype(F32).astype(BF)
    want8 = jnp.broadcast_to(wanted, (8, blocks)).astype(F32)
    rank8 = dot(want8.astype(BF), tri) * want8
    rank = rank8[0:1, :]
    spread = (
        (iota((blocks, rows), 0) == me * per + quot(iota((blocks, rows), 1), BLK))
        .astype(F32)
        .astype(BF)
    )
    for c in asks:
        c.wait_recv()
    others = asked[:, 0, :].astype(F32)
    ranks = dot(others.astype(BF), tri) * others
    places = dot(ranks.astype(BF), spread)
    srow, scol = iota((slot, rows), 0), iota((slot, rows), 1)
    same = rest(srow, BLK) == rest(scol, BLK)
    want_rank = (quot(srow, BLK) + 1).astype(F32)
    sends = []
    for k in range(1, n):
        sel = same & (jnp.broadcast_to(places[k - 1 : k, :], (slot, rows)) == want_rank)
        pick[k - 1] = dot(sel.astype(F32).astype(BF), tok[...]).astype(BF)
        c = remote(
            pick.at[k - 1],
            far.at[0, pl.ds((k - 1) * slot, slot)],
            fk_s.at[k - 1],
            fk_r.at[k - 1],
            (lax.rem(me + k, n), t),
        )
        c.start()
        sends.append(c)

    half = rows // 2

    def project(d, src, first):
        for c in loads[3 * d : 3 * d + 3]:
            c.wait()
        for j in range(3):
            for r in range(2):
                part = pl.ds(r * half, half)
                val = dot(src[part, :], wbuf[j, d])
                if first:
                    acc[j, part, :] = val
                else:
                    acc[j, part, :] += val

    project(0, tok, True)
    spots = n * slot
    col = iota((spots, blocks), 0)
    blk = iota((spots, blocks), 1)
    away = me - quot(blk, per)
    away = jnp.where(away < 0, away + n, away)
    hit = (quot(col, slot) == away - 1) & (
        jnp.broadcast_to(rank, (spots, blocks))
        == (quot(rest(col, slot), BLK) + 1).astype(F32)
    )
    hit = hit.astype(F32).astype(BF)
    far_seen = dot_nt(seen_b, hit)
    grow = (quot(iota((rows, per), 0), BLK) == iota((rows, per), 1)).astype(F32).astype(BF)
    biasf[...] = jnp.where(dot(grow, far_seen.astype(BF)) > 0.5, 0.0, NEG)
    own_seen = dot(grow, dot(seen_b, spread).astype(BF))
    causal = iota((rows, rows), 1) <= iota((rows, rows), 0)
    bias[...] = jnp.where((own_seen > 0.5) & causal, 0.0, NEG)


    own_c.wait_recv()
    project(1, gat.at[0], False)

    fwd, far_x, far_c = [], [], []

    def hand_own(c):
        own_x[c].wait_recv()
        part = pl.ds(c * piece, piece)
        f = remote(gat.at[1, part], gat.at[2, part], of_s.at[c], of_r.at[c], (me, mate))
        f.start()
        fwd.append(f)

    def hand_far(k):
        part = pl.ds((k - 1) * slot, slot)
        sends[k - 1].wait_recv()
        c = remote(far.at[0, part], far.at[2, part], fx_s.at[k - 1], fx_r.at[k - 1], (me, across))
        c.start()
        far_x.append(c)
        c = remote(far.at[0, part], far.at[1, part], fc_s.at[k - 1], fc_r.at[k - 1], (me, mate))
        c.start()
        far_c.append(c)

    for k in range(1, n):
        hand_far(k)
        at = k * OWN_CHUNKS // (n - 1)
        for c in range((k - 1) * OWN_CHUNKS // (n - 1), at):
            hand_own(c)

    project(2, gat.at[1], False)
    for f in fwd:
        f.wait_recv()
    project(3, gat.at[2], False)
    qb[...] = acc[0].astype(BF)
    kb[...] = acc[1].astype(BF)
    vb[...] = acc[2].astype(BF)

    scale = HD ** (-0.5) * LOG2E
    step = rows // 4
    cut = [slice(h * HD, (h + 1) * HD) for h in range(heads)]
    for r in range(4):
        rr = slice(r * step, (r + 1) * step)
        upto = (r + 1) * step
        shade = bias[rr, :upto]
        ss = [dot_nt(qb[rr, hc], kb[:upto, hc]) * scale + shade for hc in cut]
        ms = [jnp.max(x, axis=1, keepdims=True) for x in ss]
        ps = [jnp.exp2(x - m) for x, m in zip(ss, ms)]
        vals = [dot(p.astype(BF), vb[:upto, hc]) for p, hc in zip(ps, cut)]
        for h in range(heads):
            top[h, rr, :] = ms[h]
            tot[h, rr, :] = jnp.sum(ps[h], axis=1, keepdims=True)
            summed[h, rr, :] = vals[h]

    def project_far(d):
        for j in range(2):
            val = dot(far[d], wbuf[1 + j, d])
            if d == 0:
                accf[j] = val
            else:
                accf[j] += val

    project_far(0)
    for c in far_c:
        c.wait_recv()
    project_far(1)
    far_f = []
    used = (n - 1) * slot
    for k in range(1, n):
        part = pl.ds((k - 1) * slot, slot)
        far_x[k - 1].wait_recv()
        f = remote(far.at[2, part], far.at[3, part], ff_s.at[k - 1], ff_r.at[k - 1], (me, mate))
        f.start()
        far_f.append(f)
    project_far(2)
    for c in far_f:
        c.wait_recv()
    for j, dst in enumerate((kf, vf)):
        dst[pl.ds(0, used), :] = (accf[j] + dot(far[3], wbuf[1 + j, 3])).astype(BF)
        dst[pl.ds(used, spots - used), :] = jnp.zeros((spots - used, width), BF)

    def finish(who):
        part = pl.ds(pl.multiple_of(who * quarter, quarter), quarter)
        shade = biasf[part, :]
        ss = [dot_nt(qb[part, hc], kf[:, hc]) * scale + shade for hc in cut]
        old = [top[h, part, :] for h in range(heads)]
        ms = [jnp.maximum(m, jnp.max(x, axis=1, keepdims=True)) for m, x in zip(old, ss)]
        ps = [jnp.exp2(x - m) for x, m in zip(ss, ms)]
        keep = [jnp.exp2(m0 - m) for m0, m in zip(old, ms)]
        vals = [dot(p.astype(BF), vf[:, hc]) for p, hc in zip(ps, cut)]
        for h in range(heads):
            total = tot[h, part, :] * keep[h] + jnp.sum(ps[h], axis=1, keepdims=True)
            val = summed[h, part, :] * keep[h] + vals[h]
            att[part, cut[h]] = (val / total).astype(BF)
        return part

    wo_load.wait()
    wide = cols // OUT_CHUNKS
    to_mate, to_across = [], []

    def share(which, who):
        part = finish(who)
        for c in range(OUT_CHUNKS):
            psend[which, c] = dot(att[part, :], wobuf[:, c * wide : (c + 1) * wide]).astype(BF)
            i = which * OUT_CHUNKS + c
            x = remote(
                psend.at[which, c], precv.at[which, c], pd_s.at[i], pd_r.at[i], (me, mate)
            )
            x.start()
            to_mate.append(x)

    share(0, diag)
    part = finish(across)
    for c in range(OUT_CHUNKS):
        val = dot(att[part, :], wobuf[:, c * wide : (c + 1) * wide])
        to_mate[c].wait_recv()
        xsend[c] = (val + precv[0, c].astype(F32)).astype(BF)
        x = remote(xsend.at[c], xrecv.at[c], px_s.at[c], px_r.at[c], (me, across))
        x.start()
        to_across.append(x)
    share(1, mate)
    part = finish(t)
    for c in range(OUT_CHUNKS):
        val = dot(att[part, :], wobuf[:, c * wide : (c + 1) * wide])
        to_mate[OUT_CHUNKS + c].wait_recv()
        mine[c] = val + precv[1, c].astype(F32)
    for c in range(OUT_CHUNKS):
        to_across[c].wait_recv()
        out[:, c * wide : (c + 1) * wide] = (mine[c] + xrecv[c].astype(F32)).astype(BF)

    for c in own_x + [own_c] + asks + sends + fwd + far_x + far_c + far_f + to_mate + to_across:
        c.wait_send()


def local(n, tokens, w_query, w_key, w_value, w_out, chosen):
    rows, feat = tokens.shape
    width = w_query.shape[1]
    heads = width // HD
    cols = w_out.shape[1]
    blocks = n * (rows // BLK)
    slot = MOST * BLK
    used, spots = (n - 1) * slot, n * slot
    quarter = rows // 4
    wide = cols // OUT_CHUNKS
    vmem = pl.BlockSpec(memory_space=pltpu.VMEM)
    hbm = pl.BlockSpec(memory_space=pltpu.HBM)
    dma = pltpu.SemaphoreType.DMA
    V = pltpu.VMEM
    return pl.pallas_call(
        functools.partial(kernel, n),
        out_shape=jax.ShapeDtypeStruct((quarter, cols), BF),
        in_specs=[vmem, hbm, hbm, hbm, hbm, vmem],
        out_specs=vmem,
        scratch_shapes=[
            V((3, 4, feat, width), BF),
            V((width, cols), BF),
            V((3, rows, feat), BF),
            V((4, used, feat), BF),
            V((n - 1, slot, feat), BF),
            V((8, blocks), jnp.int32),
            V((n - 1, 8, blocks), jnp.int32),
            V((3, rows, width), F32),
            V((2, used, width), F32),
            V((rows, width), BF),
            V((rows, width), BF),
            V((rows, width), BF),
            V((spots, width), BF),
            V((spots, width), BF),
            V((rows, rows), F32),
            V((rows, spots), F32),
            V((heads, rows, 1), F32),
            V((heads, rows, 1), F32),
            V((heads, rows, HD), F32),
            V((rows, width), BF),
            V((2, OUT_CHUNKS, quarter, wide), BF),
            V((2, OUT_CHUNKS, quarter, wide), BF),
            V((OUT_CHUNKS, quarter, wide), BF),
            V((OUT_CHUNKS, quarter, wide), BF),
            V((OUT_CHUNKS, quarter, wide), F32),
            dma((13,)),
            dma((OWN_CHUNKS,)), dma((OWN_CHUNKS,)),
            dma, dma,
            dma((OWN_CHUNKS,)), dma((OWN_CHUNKS,)),
            dma((n - 1,)), dma((n - 1,)),
            dma((n - 1,)), dma((n - 1,)),
            dma((n - 1,)), dma((n - 1,)),
            dma((n - 1,)), dma((n - 1,)),
            dma((n - 1,)), dma((n - 1,)),
            dma((2 * OUT_CHUNKS,)), dma((2 * OUT_CHUNKS,)),
            dma((OUT_CHUNKS,)), dma((OUT_CHUNKS,)),
        ],
        compiler_params=pltpu.CompilerParams(
            collective_id=0, has_side_effects=True, vmem_limit_bytes=60 * 1024 * 1024
        ),
    )(tokens, w_query, w_key, w_value, w_out, chosen)


def solution(mesh):
    return jax.shard_map(
        functools.partial(local, mesh.shape["kv"]),
        mesh=mesh,
        in_specs=(
            P("kv", "tp"),
            P(None, "tp"),
            P(None, "tp"),
            P(None, "tp"),
            P("tp", None),
            P("kv", None),
        ),
        out_specs=P(("kv", "tp"), None),
        check_vma=False,
    )
```

profile of v0, /device:TPU:0, one launch (start us, length us, event | category | flops | bytes accessed | tf_op | source)
XLA Modules:
  0.0 51.4 jit_solution(8429186671043239397)
XLA Ops:
  0.0 49.5 %shard_map.64 = bf16[128,2048]{1,0:T(8,128)(2,1)} custom-call(bf16[512,512]{1,0:T(8,128)(2,1)} %tok.1, bf16[2048,384]{1,0:T(8,128)(2,1)} %wq.1, bf16[2048,384]{1,0:T(8,128)(2,1)} %wk.1, bf16[2048,384]{1,0:T(8,128)(2,1)} %wv.1, bf16[384,2048]{1,0:T(8,128)(2,1)} %wo.1, s32[16,24]{1,0:T(8,128)} %chosen.1), custom_call_target="tpu_custom_call" | custom-call | tf_op jit(solution)/shard_map/pallas_call | solution.py:334
  49.5 1.9 %copy.8 = bf16[128,2048]{1,0:T(8,128)(2,1)} copy(bf16[128,2048]{1,0:T(8,128)(2,1)} %shard_map.64) | data formatting | bytes 1048576
where the time goes:
time: 51.6 us; the launch traced here: 51.4 us
  Pallas kernels  49.5 us (96%)
  local copies, waits for them, and re-layouts  1.88 us (4%)
    pallas_call x1, Pallas kernels, local(): pl.pallas_call(functools.partial(kernel, n), out_shape=jax.ShapeDtypeStru...  49.5 us
    unnamed x1, local copies, waits for them, and re-layouts  1.88 us

commit v1 on v0

v1 whole, which is shorter than its diff:
```python
import functools

import jax
import jax.numpy as jnp
from jax import lax
from jax.experimental import pallas as pl
from jax.experimental.pallas import tpu as pltpu
from jax.sharding import PartitionSpec as P

HD = 128
BLK = 32
MOST = 2
NEG = -1e30
LOG2E = 1.4426950408889634
BF = jnp.bfloat16
F32 = jnp.float32
MESH = pl.DeviceIdType.MESH
CHUNKS = 4
OUT_CHUNKS = 4
VMEM_MIB = 60
scope = jax.named_scope


def dot(a, b):
    return jnp.dot(a, b, preferred_element_type=F32)


def dot_nt(a, b):
    return lax.dot_general(a, b, (((1,), (1,)), ((), ())), preferred_element_type=F32)


def quot(x, size):
    if size & (size - 1) == 0:
        return lax.shift_right_logical(x, jnp.full(x.shape, size.bit_length() - 1, x.dtype))
    return lax.div(x, size)


def rest(x, size):
    if size & (size - 1) == 0:
        return x & (size - 1)
    return lax.rem(x, size)


def iota(shape, dim):
    return lax.broadcasted_iota(jnp.int32, shape, dim)


def ones_where(cond):
    return cond.astype(F32).astype(BF)


def kernel(
    n, tok, wq, wk, wv, wo, chosen, out,
    rowsel, wbuf, wobuf, gat, far, pick, pickf, ask, asked, choice, qkv, kvf,
    bias, biasf, top, tot, summed, att, psend, precv, part_x, xsend, xrecv, mine,
    wsem, ox_s, ox_r, oc_s, oc_r, of_s, of_r, rq_s, rq_r, fk_s, fk_r,
    fx_s, fx_r, fc_s, fc_r, ff_s, ff_r, pd_s, pd_r, px_s, px_r,
):
    rows, feat = tok.shape
    width = wq.shape[1]
    heads = width // HD
    per = rows // BLK
    blocks = n * per
    slot = MOST * BLK
    spots = kvf.shape[0]
    cols = wo.shape[1]
    quarter = rows // 4
    piece = rows // CHUNKS
    me = lax.axis_index("kv")
    t = lax.axis_index("tp")
    mate = t + 1 - 2 * lax.rem(t, 2)
    across = lax.rem(t + 2, 4)
    diag = lax.rem(mate + 2, 4)
    last = n - 1
    near = n // 2
    reach = last - near

    def lanes(d):
        return pl.ds(pl.multiple_of(d * feat, feat), feat)

    def remote(src, dst, s, r, who):
        return pltpu.make_async_remote_copy(
            src_ref=src, dst_ref=dst, send_sem=s, recv_sem=r, device_id=who, device_id_type=MESH
        )

    barrier = pltpu.get_barrier_semaphore()
    for d in (mate, across, diag):
        pl.semaphore_signal(barrier, inc=1, device_id=(me, d), device_id_type=MESH)
    for k in range(1, n):
        pl.semaphore_signal(
            barrier, inc=1, device_id=(lax.rem(me + k, n), t), device_id_type=MESH
        )

    list_load = pltpu.make_async_copy(chosen, rowsel, wsem.at[5])
    list_load.start()
    tok_load = pltpu.make_async_copy(tok, gat.at[:, lanes(t)], wsem.at[0])
    tok_load.start()
    loads = []
    for j, w in enumerate((wq, wk, wv)):
        c = pltpu.make_async_copy(w, wbuf.at[:, pl.ds(j * width, width)], wsem.at[1 + j])
        c.start()
        loads.append(c)
    wo_load = pltpu.make_async_copy(wo, wobuf, wsem.at[4])
    wo_load.start()

    with scope("ask"):
        lane = iota((per, blocks), 1)
        seen = jnp.zeros((per, blocks), jnp.int32)
        list_load.wait()
        picks = rowsel[...]
        for j in range(picks.shape[1]):
            seen = jnp.maximum(seen, (picks[:, j : j + 1] == lane).astype(jnp.int32))
        wanted = jnp.max(seen, axis=0, keepdims=True)
        lane1 = iota((1, blocks), 1)
        inside = (lane1 >= me * per) & (lane1 < me * per + per)
        wanted = jnp.where(inside, 0, wanted).astype(F32)
        ia, ib = iota((blocks, blocks), 0), iota((blocks, blocks), 1)
        tri = ones_where((quot(ia, per) == quot(ib, per)) & (ia <= ib))
        rank = dot(jnp.broadcast_to(wanted, (8, blocks)).astype(BF), tri)[0:1, :] * wanted
        pad = max(n, 8)
        owner = quot(iota((pad, blocks), 1), per) == iota((pad, blocks), 0)
        ranks = jnp.where(owner, jnp.broadcast_to(rank, (pad, blocks)), 0.0).astype(BF)
        within = ones_where(
            rest(iota((blocks, rows), 0), per) == quot(iota((blocks, rows), 1), BLK)
        )
        places = dot(ranks, within)
        for s in range(n):
            ask[s] = jnp.broadcast_to(places[s : s + 1, :], (8, rows))

    tok_load.wait()
    with scope("barrier"):
        pl.semaphore_wait(barrier, n + 2)

    own_x, own_f = [], []
    for c in range(CHUNKS):
        part = pl.ds(c * piece, piece)
        src = gat.at[part, lanes(t)]
        own_x.append(remote(src, src, ox_s.at[c], ox_r.at[c], (me, across)))
        own_x[-1].start()
    whole = gat.at[:, lanes(t)]
    own_c = remote(whole, whole, oc_s, oc_r, (me, mate))
    own_c.start()

    asks = []
    for k in range(1, n):
        low = lax.max(me - k, 0)
        c = remote(ask.at[low], asked.at[k - 1], rq_s.at[k - 1], rq_r.at[k - 1], (low, t))
        pl.when(me >= k)(c.start)
        asks.append(c)

    with scope("bias"):
        seen_b = seen.astype(F32).astype(BF)
        spread = ones_where(iota((blocks, rows), 0) == me * per + quot(iota((blocks, rows), 1), BLK))
        col = iota((spots, blocks), 0)
        blk = iota((spots, blocks), 1)
        hit = ones_where(
            (quot(col, slot) == quot(blk, per))
            & (
                jnp.broadcast_to(rank, (spots, blocks))
                == (quot(rest(col, slot), BLK) + 1).astype(F32)
            )
        )
        far_seen = dot_nt(seen_b, hit)
        grow = ones_where(quot(iota((rows, per), 0), BLK) == iota((rows, per), 1))
        own_seen = dot(grow, dot(seen_b, spread).astype(BF))
        causal = iota((rows, rows), 1) <= iota((rows, rows), 0)
        bias[...] = jnp.where((own_seen > 0.5) & causal, 0.0, NEG)
        biasf[...] = jnp.where(dot(grow, far_seen.astype(BF)) > 0.5, 0.0, NEG)
        for s in range(last):
            part = pl.ds(s * slot, slot)
            if s < near:

                @pl.when(me <= s)
                def _():
                    far[part, :] = jnp.zeros((slot, far.shape[1]), BF)

            @pl.when(me <= s)
            def _():
                kvf[part, :] = jnp.zeros((slot, kvf.shape[1]), BF)

    with scope("picks"):
        srow, scol = iota((slot, rows), 0), iota((slot, rows), 1)
        same = rest(srow, BLK) == rest(scol, BLK)
        want_rank = (quot(srow, BLK) + 1).astype(F32)
        sends = {}

        def select(k):
            sel = same & (asked[k - 1, 0:1, :] == want_rank)
            return ones_where(sel)

        def token_send(k):
            sends[k] = remote(
                pick.at[k - 1],
                far.at[pl.ds(pl.multiple_of(lax.min(me, near - 1) * slot, slot), slot), lanes(t)],
                fk_s.at[k - 1],
                fk_r.at[me],
                (lax.rem(me + k, n), t),
            )

            @pl.when((me < near) & (me + k < n))
            def _():
                asks[k - 1].wait_recv()
                pick[k - 1] = dot(select(k), gat[:, lanes(t)]).astype(BF)
                sends[k].start()

        for k in range(last, 0, -1):
            token_send(k)

        @pl.when(me >= near)
        def _():
            for k in range(1, reach + 1):

                @pl.when(me + k < n)
                def _():
                    asks[k - 1].wait_recv()
                    choice[pl.ds((k - 1) * slot, slot), :] = select(k)

                @pl.when(me + k >= n)
                def _():
                    choice[pl.ds((k - 1) * slot, slot), :] = jnp.zeros((slot, rows), BF)

    scale = HD ** (-0.5) * LOG2E
    cut = [slice(h * HD, (h + 1) * HD) for h in range(heads)]

    def head(j, h):
        return slice(j * width + h * HD, j * width + (h + 1) * HD)

    def project(c):
        rr = slice(c * piece, (c + 1) * piece)
        val = dot(gat[rr, :], wbuf[...])
        qkv[rr, :width] = (val[:, :width] * scale).astype(BF)
        qkv[rr, width:] = val[:, width:].astype(BF)

    def attend(c):
        rr = slice(c * piece, (c + 1) * piece)
        upto = (c + 1) * piece
        shade = bias[rr, :upto]
        ss = [dot_nt(qkv[rr, head(0, h)], qkv[:upto, head(1, h)]) + shade for h in range(heads)]
        ms = [jnp.max(x, axis=1, keepdims=True) for x in ss]
        ps = [jnp.exp2(x - m) for x, m in zip(ss, ms)]
        vals = [dot(p.astype(BF), qkv[:upto, head(2, h)]) for h, p in enumerate(ps)]
        for h in range(heads):
            top[h, rr, :] = ms[h]
            tot[h, rr, :] = jnp.sum(ps[h], axis=1, keepdims=True)
            summed[h, rr, :] = vals[h]

    near_sends = []

    def send_near():
        for k in range(1, reach + 1):
            part = pl.ds((k - 1) * slot, slot)
            near_sends.append(
                remote(
                    pickf.at[part],
                    kvf.at[pl.ds(pl.multiple_of(me * slot, slot), slot)],
                    fk_s.at[k - 1],
                    fk_r.at[me],
                    (lax.rem(me + k, n), t),
                )
            )

        @pl.when((me >= near) & (me < last))
        def _():
            pickf[...] = dot(choice[...], qkv[:, width:]).astype(BF)
            for k in range(1, reach + 1):
                pl.when(me + k < n)(near_sends[k - 1].start)

    def take_near():
        for s in range(near, last):

            @pl.when(me > s)
            def _():
                here = kvf.at[slot_of(s)]
                remote(here, here, fk_s.at[0], fk_r.at[s], (me, t)).wait_recv()

    far_x, far_c, far_f = [], [], []

    def slot_of(s):
        return pl.ds(s * slot, slot)

    def hand(s):
        here = far.at[slot_of(s), lanes(t)]
        far_x.append(remote(here, here, fx_s.at[s], fx_r.at[s], (me, across)))
        far_c.append(remote(here, here, fc_s.at[s], fc_r.at[s], (me, mate)))

        @pl.when(me > s)
        def _():
            remote(pick.at[0], here, fk_s.at[0], fk_r.at[s], (me, t)).wait_recv()
            far_x[s].start()
            far_c[s].start()

    def hand_on(s):
        theirs = far.at[slot_of(s), lanes(across)]
        far_f.append(remote(theirs, theirs, ff_s.at[s], ff_r.at[s], (me, mate)))

        @pl.when(me > s)
        def _():
            far_x[s].wait_recv()
            far_f[s].start()

    def project_far(lo, hi):
        @pl.when(me > lo)
        def _():
            for s in range(lo, hi):

                @pl.when(me > s)
                def _():
                    far_c[s].wait_recv()
                    far_f[s].wait_recv()

            part = slice(lo * slot, hi * slot)
            kvf[part, :] = dot(far[part, :], wbuf[:, width:]).astype(BF)

    def absorb(part, lo, hi):
        keys = slice(lo * slot, hi * slot)
        shade = biasf[part, keys]
        ss = [dot_nt(qkv[part, head(0, h)], kvf[keys, cut[h]]) + shade for h in range(heads)]
        old = [top[h, part, :] for h in range(heads)]
        ms = [jnp.maximum(m, jnp.max(x, axis=1, keepdims=True)) for m, x in zip(old, ss)]
        ps = [jnp.exp2(x - m) for x, m in zip(ss, ms)]
        keep = [jnp.exp2(m0 - m) for m0, m in zip(old, ms)]
        vals = [dot(p.astype(BF), kvf[keys, width + h * HD : width + (h + 1) * HD]) for h, p in enumerate(ps)]
        totals = [tot[h, part, :] * keep[h] + jnp.sum(ps[h], axis=1, keepdims=True) for h in range(heads)]
        sums = [summed[h, part, :] * keep[h] + vals[h] for h in range(heads)]
        return ms, totals, sums

    def absorb_early(lo, hi):
        @pl.when(me > lo)
        def _():
            for r in range(2):
                part = slice(2 * r * quarter, 2 * (r + 1) * quarter)
                ms, totals, sums = absorb(part, lo, hi)
                for h in range(heads):
                    top[h, part, :] = ms[h]
                    tot[h, part, :] = totals[h]
                    summed[h, part, :] = sums[h]

    def finish(lo, hi, *whos):
        parts = [pl.ds(pl.multiple_of(who * quarter, quarter), quarter) for who in whos]

        @pl.when(me > lo)
        def _():
            for part in parts:
                _, totals, sums = absorb(part, lo, hi)
                for h in range(heads):
                    att[part, cut[h]] = (sums[h] / totals[h]).astype(BF)

        @pl.when(me <= lo)
        def _():
            for part in parts:
                for h in range(heads):
                    att[part, cut[h]] = (summed[h, part, :] / tot[h, part, :]).astype(BF)

        return parts

    for c in loads:
        c.wait()

    with scope("own_c"):
        own_c.wait_recv()

    def take(c):
        own_x[c].wait_recv()
        theirs = gat.at[pl.ds(c * piece, piece), lanes(across)]
        own_f.append(remote(theirs, theirs, of_s.at[c], of_r.at[c], (me, mate)))
        own_f[c].start()

    for c in range(CHUNKS):
        if c == CHUNKS - 1:
            for s in range(min(2, near)):
                with scope(f"hand{s}"):
                    hand(s)
        with scope(f"take{c}"):
            take(c)
        with scope(f"wf{c}"):
            own_f[c].wait_recv()
        with scope(f"proj{c}"):
            project(c)
        if c < CHUNKS - 1:
            with scope(f"att{c}"):
                attend(c)
    with scope("send_near"):
        send_near()
    for s in range(2, near):
        with scope(f"hand{s}"):
            hand(s)
    with scope("attlast"):
        attend(CHUNKS - 1)

    split = near // 2
    for s in range(near):
        with scope(f"on{s}"):
            hand_on(s)
        if s == split:
            with scope("pf0"):
                project_far(0, split)
            with scope("early"):
                absorb_early(0, split)
    with scope("pf1"):
        project_far(split, near)
    with scope("take_near"):
        take_near()

    with scope("wo"):
        wo_load.wait()
    wide = cols // OUT_CHUNKS
    to_mate, to_across = [], []

    def span(c):
        return slice(c * wide, (c + 1) * wide)

    def share(which, part):
        psend[which] = dot(att[part, :], wobuf[...]).astype(BF)
        for c in range(OUT_CHUNKS):
            i = which * OUT_CHUNKS + c
            x = remote(
                psend.at[which, :, span(c)],
                precv.at[which, :, span(c)],
                pd_s.at[i],
                pd_r.at[i],
                (me, mate),
            )
            x.start()
            to_mate.append(x)

    with scope("fin0"):
        first, second = finish(split, last, diag, across)
    with scope("share0"):
        share(0, first)
    with scope("sharex"):
        part_x[...] = dot(att[second, :], wobuf[...])
    with scope("sendx"):
        for c in range(OUT_CHUNKS):
            to_mate[c].wait_recv()
            xsend[:, span(c)] = (part_x[:, span(c)] + precv[0, :, span(c)].astype(F32)).astype(BF)
            here = pl.ds(0, quarter), pl.ds(c * wide, wide)
            x = remote(xsend.at[here], xrecv.at[here], px_s.at[c], px_r.at[c], (me, across))
            x.start()
            to_across.append(x)
    with scope("fin1"):
        first, second = finish(split, last, mate, t)
    with scope("share1"):
        share(1, first)
    with scope("mine"):
        mine[...] = dot(att[second, :], wobuf[...])
        for c in range(OUT_CHUNKS):
            to_mate[OUT_CHUNKS + c].wait_recv()
        mine[...] += precv[1].astype(F32)
    with scope("out"):
        for c in range(OUT_CHUNKS):
            to_across[c].wait_recv()
            out[:, span(c)] = (mine[:, span(c)] + xrecv[:, span(c)].astype(F32)).astype(BF)

    with scope("drain"):
        for c in own_x + [own_c] + own_f + to_mate + to_across:
            c.wait_send()
        for k in range(1, n):
            pl.when(me >= k)(asks[k - 1].wait_send)
            pl.when((me < near) & (me + k < n))(sends[k].wait_send)
        for k in range(1, reach + 1):
            pl.when((me >= near) & (me + k < n))(near_sends[k - 1].wait_send)
        for s in range(near):

            @pl.when(me > s)
            def _():
                far_x[s].wait_send()
                far_c[s].wait_send()
                far_f[s].wait_send()


def local(n, tokens, w_query, w_key, w_value, w_out, chosen):
    rows, feat = tokens.shape
    depth, width = w_query.shape
    heads = width // HD
    cols = w_out.shape[1]
    blocks = n * (rows // BLK)
    slot = MOST * BLK
    near = n // 2
    reach = n - 1 - near
    used = (n - 1) * slot
    quarter = rows // 4
    vmem = pl.BlockSpec(memory_space=pltpu.VMEM)
    hbm = pl.BlockSpec(memory_space=pltpu.HBM)
    dma = pltpu.SemaphoreType.DMA
    V = pltpu.VMEM
    many = dma((n - 1,))
    some = dma((CHUNKS,))
    return pl.pallas_call(
        functools.partial(kernel, n),
        out_shape=jax.ShapeDtypeStruct((quarter, cols), BF),
        in_specs=[hbm] * 6,
        out_specs=vmem,
        scratch_shapes=[
            V(chosen.shape, jnp.int32),
            V((depth, 3 * width), BF),
            V((width, cols), BF),
            V((rows, depth), BF),
            V((near * slot, depth), BF),
            V((n - 1, slot, feat), BF),
            V((reach * slot, 2 * width), BF),
            V((n, 8, rows), F32),
            V((n - 1, 8, rows), F32),
            V((reach * slot, rows), BF),
            V((rows, 3 * width), BF),
            V((used, 2 * width), BF),
            V((rows, rows), F32),
            V((rows, used), F32),
            V((heads, rows, 1), F32),
            V((heads, rows, 1), F32),
            V((heads, rows, HD), F32),
            V((rows, width), BF),
            V((2, quarter, cols), BF),
            V((2, quarter, cols), BF),
            V((quarter, cols), F32),
            V((quarter, cols), BF),
            V((quarter, cols), BF),
            V((quarter, cols), F32),
            dma((6,)),
            some, some,
            dma, dma,
            some, some,
            many, many,
            many, many,
            many, many,
            many, many,
            many, many,
            dma((2 * OUT_CHUNKS,)), dma((2 * OUT_CHUNKS,)),
            dma((OUT_CHUNKS,)), dma((OUT_CHUNKS,)),
        ],
        compiler_params=pltpu.CompilerParams(
            collective_id=0, has_side_effects=True, vmem_limit_bytes=VMEM_MIB * 1024 * 1024
        ),
    )(tokens, w_query, w_key, w_value, w_out, chosen)


def solution(mesh):
    return jax.shard_map(
        functools.partial(local, mesh.shape["kv"]),
        mesh=mesh,
        in_specs=(
            P("kv", "tp"),
            P(None, "tp"),
            P(None, "tp"),
            P(None, "tp"),
            P("tp", None),
            P("kv", None),
        ),
        out_specs=P(("kv", "tp"), None),
        check_vma=False,
    )
```

time: 51.6 us -> 46.3 us (0.90)
  the two profiles are of different devices: /device:TPU:0 before, /device:TPU:16 now
where the time goes in v1:
time: 46.3 us; the launch traced here: 46.1 us
  Pallas kernels  44.2 us (95%)
  local copies, waits for them, and re-layouts  1.88 us (4%)
    pallas_call x1, Pallas kernels, local(): pl.pallas_call(functools.partial(kernel, n), out_shape=jax.ShapeDtypeStru...  44.2 us
    unnamed x1, local copies, waits for them, and re-layouts  1.88 us

profile of v1, /device:TPU:16, one launch (start us, length us, event | category | flops | bytes accessed | tf_op | source)
XLA Modules:
  0.0 46.1 jit_solution(9004475893079587969)
XLA Ops:
  0.0 44.2 %shard_map.64 = bf16[128,2048]{1,0:T(8,128)(2,1)} custom-call(bf16[512,512]{1,0:T(8,128)(2,1)} %tok.1, bf16[2048,384]{1,0:T(8,128)(2,1)} %wq.1, bf16[2048,384]{1,0:T(8,128)(2,1)} %wk.1, bf16[2048,384]{1,0:T(8,128)(2,1)} %wv.1, bf16[384,2048]{1,0:T(8,128)(2,1)} %wo.1, s32[16,24]{1,0:T(8,128)} %chosen.1), custom_call_target="tpu_custom_call" | custom-call | tf_op jit(solution)/shard_map/pallas_call | solution.py:488
  44.2 1.9 %copy.8 = bf16[128,2048]{1,0:T(8,128)(2,1)} copy(bf16[128,2048]{1,0:T(8,128)(2,1)} %shard_map.64) | data formatting | bytes 1048576

commit v2 on v1

--- a/solution.py
+++ b/solution.py
@@ -75,6 +75,11 @@
     near = n // 2
     reach = last - near
 
+    def has(s):
+        if s >= near:
+            return me > s
+        return jnp.where(me >= near, True, (s > 0) & (me >= s))
+
     def lanes(d):
         return pl.ds(pl.multiple_of(d * feat, feat), feat)
 
@@ -125,7 +130,7 @@
         )
         places = dot(ranks, within)
         for s in range(n):
-            ask[s] = jnp.broadcast_to(places[s : s + 1, :], (8, rows))
+            ask[s] = places[s : s + 1, :]
 
     tok_load.wait()
     with scope("barrier"):
@@ -153,8 +158,13 @@
         spread = ones_where(iota((blocks, rows), 0) == me * per + quot(iota((blocks, rows), 1), BLK))
         col = iota((spots, blocks), 0)
         blk = iota((spots, blocks), 1)
+        place = quot(col, slot)
+        source = me - place
+        source = jnp.where(source < 0, source + near, source)
+        source = jnp.where(source >= near, source - near, source)
+        source = jnp.where(place < near, source, place)
         hit = ones_where(
-            (quot(col, slot) == quot(blk, per))
+            (source == quot(blk, per))
             & (
                 jnp.broadcast_to(rank, (spots, blocks))
                 == (quot(rest(col, slot), BLK) + 1).astype(F32)
@@ -168,14 +178,11 @@
         biasf[...] = jnp.where(dot(grow, far_seen.astype(BF)) > 0.5, 0.0, NEG)
         for s in range(last):
             part = pl.ds(s * slot, slot)
-            if s < near:
-
-                @pl.when(me <= s)
-                def _():
+
+            @pl.when(jnp.logical_not(has(s)))
+            def _():
+                if s < near:
                     far[part, :] = jnp.zeros((slot, far.shape[1]), BF)
-
-            @pl.when(me <= s)
-            def _():
                 kvf[part, :] = jnp.zeros((slot, kvf.shape[1]), BF)
 
     with scope("picks"):
@@ -185,26 +192,31 @@
         sends = {}
 
         def select(k):
-            sel = same & (asked[k - 1, 0:1, :] == want_rank)
+            sel = same & (asked[k - 1] == want_rank)
             return ones_where(sel)
 
-        def token_send(k):
+        for k in range(1, n):
             sends[k] = remote(
                 pick.at[k - 1],
-                far.at[pl.ds(pl.multiple_of(lax.min(me, near - 1) * slot, slot), slot), lanes(t)],
+                far.at[pl.ds(k % near * slot, slot), lanes(t)],
                 fk_s.at[k - 1],
-                fk_r.at[me],
+                fk_r.at[k % near],
                 (lax.rem(me + k, n), t),
             )
 
-            @pl.when((me < near) & (me + k < n))
+        def token_send(k, when):
+            @pl.when((me < near) & when)
             def _():
                 asks[k - 1].wait_recv()
                 pick[k - 1] = dot(select(k), gat[:, lanes(t)]).astype(BF)
                 sends[k].start()
 
-        for k in range(last, 0, -1):
-            token_send(k)
+        for j in range(near):
+            token_send(near + j, me + near + j < n)
+            if j:
+                token_send(j, me + j >= near)
+        for j in range(1, near):
+            token_send(j, me + j < near)
 
         @pl.when(me >= near)
         def _():
@@ -225,11 +237,14 @@
     def head(j, h):
         return slice(j * width + h * HD, j * width + (h + 1) * HD)
 
-    def project(c):
+    def project(c, lo, hi):
         rr = slice(c * piece, (c + 1) * piece)
-        val = dot(gat[rr, :], wbuf[...])
-        qkv[rr, :width] = (val[:, :width] * scale).astype(BF)
-        qkv[rr, width:] = val[:, width:].astype(BF)
+        val = dot(gat[rr, :], wbuf[:, lo * width : hi * width])
+        if lo == 0:
+            qkv[rr, :width] = (val[:, :width] * scale).astype(BF)
+            val = val[:, width:]
+        if hi == 3:
+            qkv[rr, width:] = val.astype(BF)
 
     def attend(c):
         rr = slice(c * piece, (c + 1) * piece)
@@ -262,7 +277,7 @@
         @pl.when((me >= near) & (me < last))
         def _():
             pickf[...] = dot(choice[...], qkv[:, width:]).astype(BF)
-            for k in range(1, reach + 1):
+            for k in range(reach, 0, -1):
                 pl.when(me + k < n)(near_sends[k - 1].start)
 
     def take_near():
@@ -283,7 +298,7 @@
         far_x.append(remote(here, here, fx_s.at[s], fx_r.at[s], (me, across)))
         far_c.append(remote(here, here, fc_s.at[s], fc_r.at[s], (me, mate)))
 
-        @pl.when(me > s)
+        @pl.when(has(s))
         def _():
             remote(pick.at[0], here, fk_s.at[0], fk_r.at[s], (me, t)).wait_recv()
             far_x[s].start()
@@ -293,17 +308,22 @@
         theirs = far.at[slot_of(s), lanes(across)]
         far_f.append(remote(theirs, theirs, ff_s.at[s], ff_r.at[s], (me, mate)))
 
-        @pl.when(me > s)
+        @pl.when(has(s))
         def _():
             far_x[s].wait_recv()
             far_f[s].start()
 
+    def any_of(lo, hi):
+        if lo >= near:
+            return me > lo
+        return (me >= near) | (me >= max(lo, 1))
+
     def project_far(lo, hi):
-        @pl.when(me > lo)
+        @pl.when(any_of(lo, hi))
         def _():
             for s in range(lo, hi):
 
-                @pl.when(me > s)
+                @pl.when(has(s))
                 def _():
                     far_c[s].wait_recv()
                     far_f[s].wait_recv()
@@ -325,7 +345,7 @@
         return ms, totals, sums
 
     def absorb_early(lo, hi):
-        @pl.when(me > lo)
+        @pl.when(any_of(lo, hi))
         def _():
             for r in range(2):
                 part = slice(2 * r * quarter, 2 * (r + 1) * quarter)
@@ -338,14 +358,14 @@
     def finish(lo, hi, *whos):
         parts = [pl.ds(pl.multiple_of(who * quarter, quarter), quarter) for who in whos]
 
-        @pl.when(me > lo)
+        @pl.when(any_of(lo, hi))
         def _():
             for part in parts:
                 _, totals, sums = absorb(part, lo, hi)
                 for h in range(heads):
                     att[part, cut[h]] = (sums[h] / totals[h]).astype(BF)
 
-        @pl.when(me <= lo)
+        @pl.when(jnp.logical_not(any_of(lo, hi)))
         def _():
             for part in parts:
                 for h in range(heads):
@@ -365,37 +385,39 @@
         own_f.append(remote(theirs, theirs, of_s.at[c], of_r.at[c], (me, mate)))
         own_f[c].start()
 
+    def step(name, act, *args):
+        with scope(name):
+            act(*args)
+
+    final = CHUNKS - 1
+    step("take0", take, 0)
     for c in range(CHUNKS):
-        if c == CHUNKS - 1:
-            for s in range(min(2, near)):
-                with scope(f"hand{s}"):
-                    hand(s)
-        with scope(f"take{c}"):
-            take(c)
-        with scope(f"wf{c}"):
-            own_f[c].wait_recv()
-        with scope(f"proj{c}"):
-            project(c)
-        if c < CHUNKS - 1:
-            with scope(f"att{c}"):
-                attend(c)
-    with scope("send_near"):
-        send_near()
-    for s in range(2, near):
-        with scope(f"hand{s}"):
-            hand(s)
-    with scope("attlast"):
-        attend(CHUNKS - 1)
+        if c == final - 2:
+            step("hand0", hand, 0)
+        if c and c < final:
+            step(f"take{c}", take, c)
+            step(f"att{c - 1}", attend, c - 1)
+        if c == final - 1:
+            step("hand1", hand, 1)
+            step(f"take{final}", take, final)
+        step(f"wf{c}", own_f[c].wait_recv)
+        if c < final:
+            step(f"proj{c}", project, c, 0, 3)
+    step("hand2", hand, 2)
+    step(f"proj{final}", project, final, 1, 3)
+    step("send_near", send_near)
+    for s in range(3, near):
+        step(f"hand{s}", hand, s)
+    step("attm", attend, final - 1)
+    step(f"projq", project, final, 0, 1)
+    step("attlast", attend, final)
 
     split = near // 2
     for s in range(near):
-        with scope(f"on{s}"):
-            hand_on(s)
+        step(f"on{s}", hand_on, s)
         if s == split:
-            with scope("pf0"):
-                project_far(0, split)
-            with scope("early"):
-                absorb_early(0, split)
+            step("pf0", project_far, 0, split)
+    step("early", absorb_early, 0, split)
     with scope("pf1"):
         project_far(split, near)
     with scope("take_near"):
@@ -461,7 +483,7 @@
             pl.when((me >= near) & (me + k < n))(near_sends[k - 1].wait_send)
         for s in range(near):
 
-            @pl.when(me > s)
+            @pl.when(has(s))
             def _():
                 far_x[s].wait_send()
                 far_c[s].wait_send()
@@ -498,8 +520,8 @@
             V((near * slot, depth), BF),
             V((n - 1, slot, feat), BF),
             V((reach * slot, 2 * width), BF),
-            V((n, 8, rows), F32),
-            V((n - 1, 8, rows), F32),
+            V((n, 1, rows), F32),
+            V((n - 1, 1, rows), F32),
             V((reach * slot, rows), BF),
             V((rows, 3 * width), BF),
             V((used, 2 * width), BF),
@@ -528,9 +550,9 @@
             dma((OUT_CHUNKS,)), dma((OUT_CHUNKS,)),
         ],
         compiler_params=pltpu.CompilerParams(
-            collective_id=0, has_side_effects=True, vmem_limit_bytes=VMEM_MIB * 1024 * 1024
+            collective_id=0, has_side_effects=True, vmem_limit_bytes=min(63, 30 + n * 3 // 2) * 1024 * 1024
         ),
-    )(tokens, w_query, w_key, w_value, w_out, chosen)
+    )(*(pltpu.with_memory_space_constraint(x, pltpu.HBM) for x in (tokens, w_query, w_key, w_value, w_out, chosen)))
 
 
 def solution(mesh):

time: 46.3 us -> 42.6 us (0.920)
  the two profiles are of different devices: /device:TPU:16 before, /device:TPU:17 now
where the time goes in v2:
time: 42.6 us; the launch traced here: 42.3 us
  Pallas kernels  41.5 us (97%)
  local copies, waits for them, and re-layouts  0.8 us (2%)
    pallas_call x1, Pallas kernels, local(): pl.pallas_call(functools.partial(kernel, n), out_shape=jax.ShapeDtypeStru...  41.5 us

profile of v2, /device:TPU:17, one launch (start us, length us, event | category | flops | bytes accessed | tf_op | source)
XLA Modules:
  0.0 42.3 jit_solution(3351886408746108494)
XLA Ops:
  0.0 41.5 %shard_map.64 = bf16[128,2048]{1,0:T(8,128)(2,1)S(1)} custom-call(bf16[512,512]{1,0:T(8,128)(2,1)} %tok.1, bf16[2048,384]{1,0:T(8,128)(2,1)} %wq.1, bf16[2048,384]{1,0:T(8,128)(2,1)} %wk.1, bf16[2048,384]{1,0:T(8,128)(2,1)} %wv.1, bf16[384,2048]{1,0:T(8,128)(2,1)} %wo.1, s32[16,24]{1,0:T(8,128)} %chosen.1), custom_call_target="tpu_custom_call" | custom-call | tf_op jit(solution)/shard_map/pallas_call | solution.py:510
  41.5 0.8 %copy.8 = bf16[128,2048]{1,0:T(8,128)(2,1)} copy(bf16[128,2048]{1,0:T(8,128)(2,1)S(1)} %shard_map.64) | data formatting | bytes 1048576
